TPU v7x, 32 devices: a whole 2x2x4 slice. The times are simulated.
32 devices in a mesh: sp: 8 (over z, x), tp: 4 (over y, core).
Axes of the slice: x: 2, y: 2, z: 4, core: 2. Of those that a mesh axis runs over, the one named last changes fastest.
Arguments:
- mixer_out: bfloat16 [1024, 2048], P('sp', 'tp'), may hold values from -12 to 12
- layer_grad: bfloat16 [1024, 2048], P('sp', 'tp'), may hold values from -6 to 6
- row_scale: float32 [1024], P('sp'), may hold values from 0.3 to 3
- norm_gain: bfloat16 [2048], replicated, may hold values from 0.099609375 to 1.8984375
- routes: int32 [1024, 2], P('sp'), may hold values from 0 to 7, all different within a row; in each aligned block of 128 rows (0 to 127, 128 to 255, ...) at most 64 rows name the same one
- route_weight: float32 [1024, 2], P('sp'), may hold values from 0.05 to 0.35
- expert_gate: bfloat16 [8, 3584, 2048], P('sp', 'tp'), may hold values from -0.125 to 0.125
- expert_up: bfloat16 [8, 3584, 2048], P('sp', 'tp'), may hold values from -0.125 to 0.125
- expert_down: bfloat16 [8, 3584, 2048], P('sp', 'tp'), may hold values from -0.09375 to 0.09375
- query_rows: bfloat16 [1024, 1024], P('sp', 'tp'), may hold values from -6 to 6
- key_rows: bfloat16 [1024, 1024], P('sp', 'tp'), may hold values from -6 to 6
- value_rows: bfloat16 [1024, 1024], P('sp', 'tp'), may hold values from -6 to 6
- retained: bfloat16 [1024, 1024], P('sp', 'tp'), may hold values from -6 to 6
- log_decay: float32 [16, 1024], P('tp', 'sp'), may hold values from -0.8 to 0
- entry_state: float32 [8, 16, 64, 64], P('sp', 'tp'), may hold values from -12 to 12
- out_proj: bfloat16 [1024, 2048], P('tp'), may hold values from -0.1875 to 0.1875
Outputs:
- grad_up: bfloat16 [8, 3584, 2048], P('sp', 'tp')
- grad_down: bfloat16 [8, 3584, 2048], P('sp', 'tp')
- grad_proj: float32 [2048, 1024], P('sp', 'tp')
- grad_query: bfloat16 [1024, 1024], P('sp', 'tp')
- grad_key: bfloat16 [1024, 1024], P('sp', 'tp')
- grad_value: bfloat16 [1024, 1024], P('sp', 'tp')
- stream_grad: bfloat16 [1024, 2048], P('sp', 'tp')
Inputs may be any that keep to these rules, and one draw needn't show every extreme that they name: `routes`: each row names 2 different experts. Among the entries of one block of 128 consecutive rows no expert appears more than 64 times, and in every draw some block names some expert exactly 64 times.
All inputs are finite; a program needn't handle non-finite values.
Results may differ from a plain program's by a relative error of at most 0.025.
Values may be sent and summed in bfloat16 or wider, within the bound.
A program may use at most 64 MiB of HBM per device.

v0:
```python
import jax
import jax.numpy as jnp
from jax import lax
from jax.sharding import PartitionSpec as P


def prefix(array, axis, combine, identity):
    devices, position = (lax.axis_size(axis), lax.axis_index(axis))
    everything = jax.tree.map(lambda part: lax.all_gather(part, axis), array)
    start = jax.tree.map(
        lambda part, zero: jnp.broadcast_to(jnp.asarray(zero, part.dtype), part.shape),
        array,
        identity,
    )

    def step(k, before):
        at = devices - 1 - k
        reached = at > position
        new = combine(before, jax.tree.map(lambda part: part[at], everything))
        return jax.tree.map(lambda a, b: jnp.where(reached, a, b), new, before)

    return lax.fori_loop(0, devices, step, start)


def contract_last(first_op, second_op):
    return lax.dot_general(
        first_op, second_op, (((1,), (1,)), ((), ())), preferred_element_type=jnp.float32
    )


def contract_first(first_op, second_op):
    return lax.dot_general(
        first_op, second_op, (((0,), (0,)), ((), ())), preferred_element_type=jnp.float32
    )


def slot_sources(routes, experts, capacity):
    flat_ids = routes.reshape(-1)
    entries = flat_ids.shape[0]
    onehot = (flat_ids[:, None] == jnp.arange(experts, dtype=jnp.int32)[None, :]).astype(jnp.int32)
    rank_in = jnp.sum(onehot * (jnp.cumsum(onehot, axis=0) - 1), axis=1)
    slot_ids = flat_ids * capacity + rank_in
    matches = slot_ids[None, :] == jnp.arange(experts * capacity, dtype=jnp.int32)[:, None]
    sources = jnp.sum(jnp.where(matches, jnp.arange(entries, dtype=jnp.int32)[None, :], 0), axis=1)
    sources = jnp.where(jnp.any(matches, axis=1), sources, entries)
    return (slot_ids, sources)


def pick_rows(row_block, sources):
    padded = jnp.concatenate(
        [row_block, jnp.zeros((1, row_block.shape[1]), row_block.dtype)], axis=0
    )
    return jnp.take(padded, sources, axis=0)


def span_terms(head_queries, head_keys, head_values, head_gradient, decay_head, incoming_state):
    scale = head_queries.shape[-1] ** (-0.5)
    length = decay_head.shape[1]
    cumul = jnp.cumsum(decay_head, axis=1)
    places = jnp.arange(length)
    causal = (places[:, None] >= places[None, :])[None, :, :]
    spread = cumul[:, :, None] - cumul[:, None, :]
    weights = jnp.where(causal, jnp.exp(jnp.where(causal, spread, 0.0)), 0.0)
    scores = (
        scale
        * jnp.einsum("thd,shd->hts", head_queries, head_keys, precision=lax.Precision.HIGHEST)
        * weights
    )
    pressure = (
        scale
        * jnp.einsum("thd,shd->hts", head_gradient, head_values, precision=lax.Precision.HIGHEST)
        * weights
    )
    grad_query = jnp.einsum("hts,shd->thd", pressure, head_keys, precision=lax.Precision.HIGHEST)
    grad_key = jnp.einsum("hts,thd->shd", pressure, head_queries, precision=lax.Precision.HIGHEST)
    grad_value = jnp.einsum("hts,thd->shd", scores, head_gradient, precision=lax.Precision.HIGHEST)
    ascending_decay = jnp.exp(cumul).T
    grad_query = grad_query + scale * ascending_decay[:, :, None] * jnp.einsum(
        "joy,oiy->joi", head_gradient, incoming_state, precision=lax.Precision.HIGHEST
    )
    state_update = jnp.einsum(
        "olb,oli->lbi",
        head_queries * ascending_decay[:, :, None],
        head_gradient,
        precision=lax.Precision.HIGHEST,
    )
    survive = jnp.exp(cumul[:, -1])
    falling = jnp.exp(cumul[:, -1:] - cumul).T
    return (grad_query, grad_key, grad_value, state_update, survive, falling)


def add_carried(grad_key, grad_value, head_keys, head_values, falling, carried_over_state):
    scale = head_keys.shape[-1] ** (-0.5)
    grad_key = grad_key + scale * falling[:, :, None] * jnp.einsum(
        "upy,ruy->rup", carried_over_state, head_values, precision=lax.Precision.HIGHEST
    )
    grad_value = grad_value + scale * falling[:, :, None] * jnp.einsum(
        "rzw,erz->erw", carried_over_state, head_keys, precision=lax.Precision.HIGHEST
    )
    return (grad_key, grad_value)


def combine_spans(earlier, later_run):
    return (later_run[0] * earlier[0], later_run[1] + later_run[0][:, None, None] * earlier[1])


def body(
    mixer_out,
    layer_grad,
    row_scale,
    norm_gain,
    routes,
    route_weight,
    expert_gate,
    expert_up,
    expert_down,
    query_rows,
    key_rows,
    value_rows,
    retained,
    log_decay,
    entry_state,
    out_proj,
):
    experts = lax.axis_size("sp")
    tp_count = lax.axis_size("tp")
    tokens_here, columns = mixer_out.shape
    fanout = routes.shape[1]
    capacity = 2 * fanout * tokens_here // experts
    slot_ids, sources = slot_sources(routes, experts, capacity)
    gain_all = norm_gain.astype(jnp.float32)
    gain_cols = lax.dynamic_slice_in_dim(gain_all, lax.axis_index("tp") * columns, columns)
    scaled = mixer_out.astype(jnp.float32) * row_scale[:, None]
    normed = (scaled * gain_cols[None, :]).astype(jnp.bfloat16)
    weight_col = route_weight.reshape(-1)[:, None]
    weighted = (weight_col * jnp.repeat(layer_grad.astype(jnp.float32), fanout, axis=0)).astype(
        jnp.bfloat16
    )
    send_normed = pick_rows(jnp.repeat(normed, fanout, axis=0), sources).reshape(
        experts, capacity, columns
    )
    send_grad = pick_rows(weighted, sources).reshape(experts, capacity, columns)
    got_normed, got_grad = (
        lax.all_to_all(send_normed, "sp", split_axis=0, concat_axis=0, tiled=True),
        lax.all_to_all(send_grad, "sp", split_axis=0, concat_axis=0, tiled=True),
    )
    gate_weight = expert_gate[0]
    up_weight = expert_up[0]
    down_weight = expert_down[0]
    model_width = gate_weight.shape[1]
    full_normed, full_grad = (
        lax.all_gather(got_normed, "tp", axis=2, tiled=True),
        lax.all_gather(got_grad, "tp", axis=2, tiled=True),
    )
    normed_rows = full_normed.reshape(-1, model_width)
    grad_rows = full_grad.reshape(-1, model_width)
    gate_pre = contract_last(normed_rows, gate_weight)
    up_pre = contract_last(normed_rows, up_weight)
    act_grad = contract_last(grad_rows, down_weight)
    sigmoid_gate = jax.nn.sigmoid(gate_pre)
    silu_gate = gate_pre * sigmoid_gate
    activation = (silu_gate * up_pre).astype(jnp.bfloat16)
    grad_down = contract_first(activation, grad_rows).astype(jnp.bfloat16)[None]
    up_grad = (act_grad * silu_gate).astype(jnp.bfloat16)
    gate_grad = (act_grad * up_pre * sigmoid_gate * (1.0 + gate_pre * (1.0 - sigmoid_gate))).astype(
        jnp.bfloat16
    )
    grad_up = contract_first(up_grad, normed_rows).astype(jnp.bfloat16)[None]
    partial_value = jnp.dot(gate_grad, gate_weight, preferred_element_type=jnp.float32) + jnp.dot(
        up_grad, up_weight, preferred_element_type=jnp.float32
    )
    shares = lax.psum_scatter(
        partial_value.astype(jnp.bfloat16), "tp", scatter_dimension=1, tiled=True
    )
    returned = lax.all_to_all(
        shares.reshape(experts, capacity, columns), "sp", split_axis=0, concat_axis=0, tiled=True
    )
    per_route = jnp.take(returned.reshape(experts * capacity, columns), slot_ids, axis=0)
    hidden_grad = jnp.sum(
        per_route.reshape(tokens_here, fanout, columns).astype(jnp.float32), axis=1
    ).astype(jnp.bfloat16)
    attend = gain_cols[None, :] * hidden_grad.astype(jnp.float32)
    total_dot = lax.psum(jnp.sum(scaled * attend, axis=1), "tp")
    mean_dot = total_dot[:, None] / (columns * tp_count)
    stream_grad = (
        layer_grad.astype(jnp.float32) + row_scale[:, None] * (attend - scaled * mean_dot)
    ).astype(jnp.bfloat16)
    stream_full = lax.all_gather(stream_grad, "tp", axis=1, tiled=True)
    out_grad = contract_last(stream_full, out_proj).astype(jnp.bfloat16)
    head_count = entry_state.shape[1]
    head_dim = entry_state.shape[-1]

    def split_heads(block):
        return block.astype(jnp.float32).reshape(tokens_here, head_count, head_dim)

    head_keys = split_heads(key_rows)
    head_values = split_heads(value_rows)
    grad_query, grad_key, grad_value, state_update, survive, falling = span_terms(
        split_heads(query_rows),
        head_keys,
        head_values,
        split_heads(out_grad),
        log_decay,
        entry_state[0],
    )
    carried_over_state = prefix(
        (survive, state_update),
        "sp",
        combine_spans,
        (jnp.ones_like(survive), jnp.zeros_like(state_update)),
    )[1]
    grad_key, grad_value = add_carried(
        grad_key, grad_value, head_keys, head_values, falling, carried_over_state
    )
    grad_proj = lax.psum_scatter(
        contract_first(stream_full, retained).astype(jnp.bfloat16),
        "sp",
        scatter_dimension=0,
        tiled=True,
    ).astype(jnp.float32)
    ret_cols = head_count * head_dim
    return (
        grad_up,
        grad_down,
        grad_proj,
        grad_query.reshape(tokens_here, ret_cols).astype(jnp.bfloat16),
        grad_key.reshape(tokens_here, ret_cols).astype(jnp.bfloat16),
        grad_value.reshape(tokens_here, ret_cols).astype(jnp.bfloat16),
        stream_grad,
    )


def solution(mesh):
    in_specs = (
        P("sp", "tp"),
        P("sp", "tp"),
        P("sp"),
        P(),
        P("sp", None),
        P("sp", None),
        P("sp", "tp", None),
        P("sp", "tp", None),
        P("sp", "tp", None),
        P("sp", "tp"),
        P("sp", "tp"),
        P("sp", "tp"),
        P("sp", "tp"),
        P("tp", "sp"),
        P("sp", "tp", None, None),
        P("tp", None),
    )
    out_specs = (
        P("sp", "tp", None),
        P("sp", "tp", None),
        P("sp", "tp"),
        P("sp", "tp"),
        P("sp", "tp"),
        P("sp", "tp"),
        P("sp", "tp"),
    )
    return jax.shard_map(body, mesh=mesh, in_specs=in_specs, out_specs=out_specs, check_vma=False)
```

profile of v0, /device:TPU:0, one launch (start us, length us, event | category | flops | bytes accessed | tf_op | source)
XLA Modules:
  0.0 272.4 jit_solution(12463252049788378154)
XLA Ops:
  13.6 2.0 gather_fusion.2
  15.5 2.0 gather_fusion.1
  17.7 21.7 %all_to_all.15 = bf16[8,64,512]{2,1,0:T(8,128)(2,1)} all-to-all(bf16[8,64,512]{2,1,0:T(8,128)(2,1)S(1)} %bitcast.123), channel_id=1, replica_groups=mesh['sp'=8,'tp'=4] {'sp'}, dimensions={0} | all-to-all | bytes 1048576 | tf_op jit(solution)/shard_map/all_to_all | solution.py:144
  39.5 17.6 %all_to_all.16 = bf16[8,64,512]{2,1,0:T(8,128)(2,1)} all-to-all(bf16[8,64,512]{2,1,0:T(8,128)(2,1)S(1)} %bitcast.122), channel_id=1, replica_groups=mesh['sp'=8,'tp'=4] {'sp'}, dimensions={0} | all-to-all | bytes 1048576 | tf_op jit(solution)/shard_map/all_to_all | solution.py:145
  57.4 3.8 %all-gather.7.cloned.1.call-done = bf16[8,64,2048]{2,1,0:T(8,128)(2,1)} async-done(((bf16[8,64,512]{2,1,0:T(8,128)(2,1)}), bf16[8,64,2048]{2,1,0:T(8,128)(2,1)}) %all-gather.7.cloned.1.call-update) | async-done | bytes 2097168 | tf_op jit(solution)/shard_map/all_gather | solution.py:152
  61.2 6.4 %fusion.7 = f32[512,896]{1,0:T(8,128)} fusion(bf16[512,2048]{1,0:T(8,128)(2,1)} %bitcast.142, bf16[1,896,2048]{2,1,0:T(8,128)(2,1)} %param.26), kind=kOutput, calls=%fused_computation.13 | convolution fusion | flops 1879048192 | bytes 7602176 | tf_op jit(solution)/shard_map/dot_general | solution.py:26
  67.6 3.6 %fusion.3 = f32[512,896]{1,0:T(8,128)} fusion(bf16[512,2048]{1,0:T(8,128)(2,1)S(1)} %bitcast.144, bf16[1,896,2048]{2,1,0:T(8,128)(2,1)S(1)} %copy-done.13), kind=kOutput, calls=%fused_computation.9 | convolution fusion | flops 1879048192 | bytes 7602176 | tf_op jit(solution)/shard_map/dot_general | solution.py:26
  71.3 14.1 %all-gather.5.cloned.1.call-done = bf16[8,64,2048]{2,1,0:T(8,128)(2,1)} async-done(((bf16[8,64,512]{2,1,0:T(8,128)(2,1)}), bf16[8,64,2048]{2,1,0:T(8,128)(2,1)}) %all-gather.5.cloned.1.call-update) | async-done | bytes 2097168 | tf_op jit(solution)/shard_map/all_gather | solution.py:153
  85.3 5.8 %multiply_convert_fusion.2 = (bf16[512,896]{1,0:T(8,128)(2,1)S(1)}, f32[512,896]{1,0:T(8,128)S(1)}) fusion(f32[512,896]{1,0:T(8,128)} %fusion.7, bf16[512,2048]{1,0:T(8,128)(2,1)} %bitcast.145, bf16[1,896,2048]{2,1,0:T(8,128)(2,1)} %param.28), kind=kOutput, calls=%fused_computation.22 | convolution fusion | flops 1881800704 | bytes 10354688 | tf_op jit(solution)/shard_map/dot_general | solution.py:26
  91.2 2.3 fusion.1
  94.6 4.1 %add_convert_fusion = bf16[512,2048]{1,0:T(8,128)(2,1)} fusion(f32[512,2048]{1,0:T(8,128)S(1)} %fusion.1, bf16[1,896,2048]{2,1,0:T(8,128)(2,1)S(1)} %copy-done.15, f32[512,896]{1,0:T(8,128)S(1)} %copy-done.19, f32[512,896]{1,0:T(8,128)S(1)} %get-tuple-element.213, f32[512,896]{1,0:T(8,128)S(1)} %copy-done.21), kind=kOutput, calls=%fused_computation.6 | convolution fusion | flops 1885732864 | bytes 15466496 | tf_op jit(solution)/shard_map/dot_general | solution.py:169
  102.1 21.3 %all-reduce.2 = f32[32]{0:T(128)S(1)} all-reduce(f32[32]{0:T(128)S(1)} %dynamic-update-slice), channel_id=3, replica_groups=mesh['sp'=8,'tp'=4] {'sp'}, use_global_device_ids=true, to_apply=%add.2 | all-reduce | flops 32 | bytes 256
  124.1 6.0 %reduce-scatter.3.cloned.1.call-done = bf16[512,512]{1,0:T(8,128)(2,1)} async-done(((bf16[512,2048]{1,0:T(8,128)(2,1)}), bf16[512,512]{1,0:T(8,128)(2,1)}) %reduce-scatter.3.cloned.1.call-update) | async-done | bytes 524304 | tf_op jit(solution)/shard_map/reduce_scatter | solution.py:172
  130.2 5.5 %all-to-all-start.2 = ((bf16[8,64,512]{2,1,0:T(8,128)(2,1)}), bf16[8,64,512]{2,1,0:T(8,128)(2,1)S(1)}, u32[]{:S(2)}, u32[]{:S(2)}) async-start(bf16[8,64,512]{2,1,0:T(8,128)(2,1)} %bitcast.134), calls=%async_computation.3 | async-start | bytes 1048576 | tf_op jit(solution)/shard_map/all_to_all | solution.py:175
  136.0 6.0 %convert_bitcast_fusion.1 = bf16[1,896,2048]{2,1,0:T(8,128)(2,1)} fusion(bf16[512,896]{1,0:T(8,128)(2,1)} %copy-done.23, bf16[512,2048]{1,0:T(8,128)(2,1)} %bitcast.143), kind=kOutput, calls=%fused_computation.18 | convolution fusion | flops 1880883200 | bytes 6684672 | tf_op jit(solution)/shard_map/dot_general | solution.py:32
  141.9 4.0 %convert_bitcast_fusion = bf16[1,896,2048]{2,1,0:T(8,128)(2,1)} fusion(bf16[512,2048]{1,0:T(8,128)(2,1)S(1)} %bitcast.146, f32[512,896]{1,0:T(8,128)S(1)} %copy-done.22, f32[512,896]{1,0:T(8,128)S(1)} %copy-done.20), kind=kOutput, calls=%fused_computation.17 | convolution fusion | flops 1883635712 | bytes 9437184 | tf_op jit(solution)/shard_map/dot_general | solution.py:32
  145.9 4.1 %all-to-all-done.2 = bf16[8,64,512]{2,1,0:T(8,128)(2,1)S(1)} async-done(((bf16[8,64,512]{2,1,0:T(8,128)(2,1)}), bf16[8,64,512]{2,1,0:T(8,128)(2,1)S(1)}, u32[]{:S(2)}, u32[]{:S(2)}) %all-to-all-start.2) | async-done | bytes 524320 | tf_op jit(solution)/shard_map/all_to_all | solution.py:175
  150.0 1.2 gather_fusion
  152.1 5.9 %psum.7 = f32[128]{0:T(128)S(1)} all-reduce(f32[128]{0:T(128)S(1)} %multiply_reduce_fusion), channel_id=1, replica_groups=mesh['sp'=8,'tp'=4] {'tp'}, use_global_device_ids=true, to_apply=%region_8.10 | all-reduce | flops 128 | bytes 1024 | tf_op jit(solution)/shard_map/psum | solution.py:183
  158.2 6.5 %all_gather.21 = bf16[128,2048]{1,0:T(8,128)(2,1)S(1)} all-gather(bf16[128,512]{1,0:T(8,128)(2,1)S(1)} %add_convert_fusion.1), channel_id=1, replica_groups=mesh['sp'=8,'tp'=4] {'tp'}, dimensions={1}, use_global_device_ids=true | all-gather | bytes 655360 | tf_op jit(solution)/shard_map/all_gather | solution.py:188
  165.6 32.8 %all-gather = f32[32,64,64]{2,1,0:T(8,128)S(1)} all-gather(f32[4,64,64]{2,1,0:T(8,128)S(1)} %fusion.30), channel_id=2, replica_groups=mesh['sp'=8,'tp'=4] {'sp'}, dimensions={0}, use_global_device_ids=true | all-gather | bytes 589824 | tf_op jit(solution)/shard_map/all_gather | solution.py:9
  198.4 1.5 convolution_convert_fusion
  205.1 59.2 %reduce-scatter.5.cloned.1.call-done = bf16[256,256]{1,0:T(8,128)(2,1)} async-done(((bf16[2048,256]{1,0:T(8,128)(2,1)}), bf16[256,256]{1,0:T(8,128)(2,1)}) %reduce-scatter.5.cloned.1.call-update) | async-done | bytes 131088 | tf_op jit(solution)/shard_map/reduce_scatter | solution.py:215
  264.3 1.6 convert_element_type.93
  (140 shorter events, 19.2 us)
Async XLA Ops:
  7.2 157.6 %copy-start = (bf16[256,2048]{1,0:T(8,128)(2,1)S(1)}, bf16[256,2048]{1,0:T(8,128)(2,1)}, u32[]{:S(2)}) copy-start(bf16[256,2048]{1,0:T(8,128)(2,1)} %param.35) | copy-start | bytes 3145732
  7.2 6.0 %copy-start.12 = (f32[128,2]{0,1:T(2,128)S(1)}, f32[128,2]{0,1:T(2,128)}, u32[]{:S(2)}) copy-start(f32[128,2]{0,1:T(2,128)} %param.25) | copy-start | bytes 3076
  7.2 54.0 %all-gather.7.cloned.1.call-start = ((), (), s32[]{:S(2)}) async-start(), calls=%async_computation.6 | async-start | bytes 2621440 | tf_op jit(solution)/shard_map/all_gather | solution.py:152
  39.4 45.9 %all-gather.5.cloned.1.call-start = ((), (), s32[]{:S(2)}) async-start(), calls=%async_computation.5 | async-start | bytes 2621440 | tf_op jit(solution)/shard_map/all_gather | solution.py:153
  57.1 73.0 %reduce-scatter.3.cloned.1.call-start = ((), (), s32[]{:S(2)}) async-start(), calls=%async_computation.7 | async-start | bytes 2621440 | tf_op jit(solution)/shard_map/reduce_scatter | solution.py:172
  61.2 6.5 %copy-start.13 = (bf16[1,896,2048]{2,1,0:T(8,128)(2,1)S(1)}, bf16[1,896,2048]{2,1,0:T(8,128)(2,1)}, u32[]{:S(2)}) copy-start(bf16[1,896,2048]{2,1,0:T(8,128)(2,1)} %param.27) | copy-start | bytes 11010052
  61.2 6.5 %copy-start.16 = (bf16[8,64,2048]{2,1,0:T(8,128)(2,1)S(1)}, bf16[8,64,2048]{2,1,0:T(8,128)(2,1)}, u32[]{:S(2)}) copy-start(bf16[8,64,2048]{2,1,0:T(8,128)(2,1)} %all-gather.7.cloned.1.call-done) | copy-start | bytes 6291460
  85.3 5.8 %copy-start.14 = (bf16[1,896,2048]{2,1,0:T(8,128)(2,1)S(1)}, bf16[1,896,2048]{2,1,0:T(8,128)(2,1)}, u32[]{:S(2)}) copy-start(bf16[1,896,2048]{2,1,0:T(8,128)(2,1)} %param.27) | copy-start | bytes 11010052
  91.1 2.4 copy-start.23
  91.2 2.9 %copy-start.19 = (f32[512,896]{1,0:T(8,128)S(1)}, f32[512,896]{1,0:T(8,128)}, u32[]{:S(2)}) copy-start(f32[512,896]{1,0:T(8,128)} %fusion.7) | copy-start | bytes 5505028
  91.2 3.5 %copy-start.21 = (f32[512,896]{1,0:T(8,128)S(1)}, f32[512,896]{1,0:T(8,128)}, u32[]{:S(2)}) copy-start(f32[512,896]{1,0:T(8,128)} %fusion.3) | copy-start | bytes 5505028
  98.8 24.7 %copy-start.7 = (bf16[128,256]{1,0:T(8,128)(2,1)S(1)}, bf16[128,256]{1,0:T(8,128)(2,1)}, u32[]{:S(2)}) copy-start(bf16[128,256]{1,0:T(8,128)(2,1)} %param.30) | copy-start | bytes 196612
  98.8 24.8 %copy-start.8 = (bf16[128,256]{1,0:T(8,128)(2,1)S(1)}, bf16[128,256]{1,0:T(8,128)(2,1)}, u32[]{:S(2)}) copy-start(bf16[128,256]{1,0:T(8,128)(2,1)} %param.31) | copy-start | bytes 196612
  130.2 19.8 %all-to-all-start.2 = ((bf16[8,64,512]{2,1,0:T(8,128)(2,1)}), bf16[8,64,512]{2,1,0:T(8,128)(2,1)S(1)}, u32[]{:S(2)}, u32[]{:S(2)}) async-start(bf16[8,64,512]{2,1,0:T(8,128)(2,1)} %bitcast.134), calls=%async_computation.3 | async-start | bytes 1048576 | tf_op jit(solution)/shard_map/all_to_all | solution.py:175
  135.7 128.6 %reduce-scatter.5.cloned.1.call-start = ((), (), s32[]{:S(2)}) async-start(), calls=%async_computation.8 | async-start | bytes 1179648 | tf_op jit(solution)/shard_map/reduce_scatter | solution.py:215
  135.9 6.0 %copy-start.17 = (bf16[8,64,2048]{2,1,0:T(8,128)(2,1)S(1)}, bf16[8,64,2048]{2,1,0:T(8,128)(2,1)}, u32[]{:S(2)}) copy-start(bf16[8,64,2048]{2,1,0:T(8,128)(2,1)} %all-gather.5.cloned.1.call-done) | copy-start | bytes 6291460
  135.9 6.0 %copy-start.20 = (f32[512,896]{1,0:T(8,128)S(1)}, f32[512,896]{1,0:T(8,128)}, u32[]{:S(2)}) copy-start(f32[512,896]{1,0:T(8,128)} %fusion.7) | copy-start | bytes 5505028
  136.0 6.0 %copy-start.22 = (f32[512,896]{1,0:T(8,128)S(1)}, f32[512,896]{1,0:T(8,128)}, u32[]{:S(2)}) copy-start(f32[512,896]{1,0:T(8,128)} %fusion.3) | copy-start | bytes 5505028
  145.9 6.0 %copy-start.1 = (bf16[128,512]{1,0:T(8,128)(2,1)S(1)}, bf16[128,512]{1,0:T(8,128)(2,1)}, u32[]{:S(2)}) copy-start(bf16[128,512]{1,0:T(8,128)(2,1)} %param.20) | copy-start | bytes 393220
  145.9 6.0 %copy-start.10 = (f32[128]{0:T(128)S(1)}, f32[128]{0:T(128)}, u32[]{:S(2)}) copy-start(f32[128]{0:T(128)} %param.22) | copy-start | bytes 1540
  145.9 12.1 %copy-start.2 = (bf16[128,512]{1,0:T(8,128)(2,1)S(1)}, bf16[128,512]{1,0:T(8,128)(2,1)}, u32[]{:S(2)}) copy-start(bf16[128,512]{1,0:T(8,128)(2,1)} %param.21) | copy-start | bytes 393220
  158.0 40.3 %copy-start.5 = (bf16[128,256]{1,0:T(8,128)(2,1)S(1)}, bf16[128,256]{1,0:T(8,128)(2,1)}, u32[]{:S(2)}) copy-start(bf16[128,256]{1,0:T(8,128)(2,1)} %param.32) | copy-start | bytes 196612
  158.2 41.6 %copy-start.3 = (bf16[128,512]{1,0:T(8,128)(2,1)}, bf16[128,512]{1,0:T(8,128)(2,1)S(1)}, u32[]{:S(2)}) copy-start(bf16[128,512]{1,0:T(8,128)(2,1)S(1)} %add_convert_fusion.1) | copy-start | bytes 393220
  199.9 3.9 %copy-start.4 = (f32[1,4,64,64]{3,2,1,0:T(8,128)S(1)}, f32[1,4,64,64]{3,2,1,0:T(8,128)}, u32[]{:S(2)}) copy-start(f32[1,4,64,64]{3,2,1,0:T(8,128)} %param.34) | copy-start | bytes 196612
  (5 other events, 7.2 us)
Sparse Core Ops, SparseCore 0:
  39.6 21.5 all-gather.6
  62.7 22.5 all-gather.4
  98.9 31.1 reduce-scatter.2
  200.0 64.2 reduce-scatter.4
where the time goes:
time: 273 us; the launch traced here: 272 us
  blocking collectives  106 us (39%)
  waiting for transfers between devices  87.3 us (32%)
  matrix products  36.5 us (13%)
  between operations  15 us (5%)
  local copies, waits for them, and re-layouts  14.6 us (5%)
  other arithmetic  6.82 us (2%)
  starting transfers between devices  6.07 us (2%)
    reduce_scatter x1, waiting for transfers between devices, body(): lax.psum_scatter(contract_first(stream_full, retained).astype(jnp.bfloat1...  59.2 us
    all_gather x1, blocking collectives, prefix(): everything = jax.tree.map(lambda part: lax.all_gather(part, axis), array)  32.8 us
    all_to_all x1, blocking collectives, body(): lax.all_to_all(send_normed, 'sp', split_axis=0, concat_axis=0, tiled=True)  21.7 us
    unnamed x1, blocking collectives  21.3 us
    all_to_all x1, blocking collectives, body(): lax.all_to_all(send_grad, 'sp', split_axis=0, concat_axis=0, tiled=True)  17.6 us
    dot_general x4, matrix products, contract_last(): lax.dot_general(first_op, second_op, (((1,), (1,)), ((), ())), preferred_...  16.3 us
    all_gather x1, waiting for transfers between devices, body(): lax.all_gather(got_grad, 'tp', axis=2, tiled=True)  14.1 us
    dot_general x3, matrix products, contract_first(): lax.dot_general(first_op, second_op, (((0,), (0,)), ((), ())), preferred_...  11.4 us
  transfers between devices with their start and end apart: 5, of which 5 were waited for; matrix products, arithmetic and copies ran while one was open for 10% of the time, Pallas kernels for 0%

commit v1 on v0

--- a/solution.py
+++ b/solution.py
@@ -150,7 +150,7 @@
     model_width = gate_weight.shape[1]
     full_normed, full_grad = (
         lax.all_gather(got_normed, "tp", axis=2, tiled=True),
-        lax.all_gather(got_grad, "tp", axis=2, tiled=True),
+        jnp.concatenate(lax.all_gather(got_grad, "tp"), axis=2),
     )
     normed_rows = full_normed.reshape(-1, model_width)
     grad_rows = full_grad.reshape(-1, model_width)

time: 273 us -> 276 us (1.011)
  matrix products: 36.5 us -> 30.6 us
  waiting for transfers between devices: 87.3 us -> 92.7 us
  local copies, waits for them, and re-layouts: 14.6 us -> 17.7 us
    all_gather x1, waiting for transfers between devices: 3.82 us -> 20.3 us  [body(): lax.all_gather(got_normed, 'tp', axis=2, tiled=True)]
    all_gather x1, waiting for transfers between devices: 14.1 us -> 3.82 us  [body(): lax.all_gather(got_grad, 'tp')]
    dot_general x4, matrix products: 16.3 us -> 10.5 us  [contract_last(): lax.dot_general(first_op, second_op, (((1,), (1,)), ((), ())), preferred_...]
    all_to_all x1, blocking collectives: 17.6 us -> 21.7 us  [body(): lax.all_to_all(send_grad, 'sp', split_axis=0, concat_axis=0, tiled=True)]
    all_to_all x1, blocking collectives: 21.7 us -> 17.6 us  [body(): lax.all_to_all(send_normed, 'sp', split_axis=0, concat_axis=0, tiled=True)]
    reshape x0 -> x1, local copies, waits for them, and re-layouts: none -> 3.21 us  [body(): jnp.concatenate(lax.all_gather(got_grad, 'tp'), axis=2)]
    unnamed x59 -> x62, local copies, waits for them, and re-layouts: 6.02 us -> 5.82 us
  transfers between devices with their start and end apart: 5 -> 5, of which waited for: 5 -> 5; matrix products, arithmetic and copies ran while one was open for 10% -> 8% of each run, Pallas kernels for 0% -> 0%
where the time goes in v1:
time: 276 us; the launch traced here: 275 us
  blocking collectives  106 us (38%)
  waiting for transfers between devices  92.7 us (34%)
  matrix products  30.6 us (11%)
  local copies, waits for them, and re-layouts  17.7 us (6%)
  between operations  15 us (5%)
  other arithmetic  6.82 us (2%)
  starting transfers between devices  5.84 us (2%)
    reduce_scatter x1, waiting for transfers between devices, body(): lax.psum_scatter(contract_first(stream_full, retained).astype(jnp.bfloat1...  58.3 us
    all_gather x1, blocking collectives, prefix(): everything = jax.tree.map(lambda part: lax.all_gather(part, axis), array)  32.9 us
    all_to_all x1, blocking collectives, body(): lax.all_to_all(send_grad, 'sp', split_axis=0, concat_axis=0, tiled=True)  21.7 us
    unnamed x1, blocking collectives  21.3 us
    all_gather x1, waiting for transfers between devices, body(): lax.all_gather(got_normed, 'tp', axis=2, tiled=True)  20.3 us
    all_to_all x1, blocking collectives, body(): lax.all_to_all(send_normed, 'sp', split_axis=0, concat_axis=0, tiled=True)  17.6 us
    dot_general x3, matrix products, contract_first(): lax.dot_general(first_op, second_op, (((0,), (0,)), ((), ())), preferred_...  11.4 us
    dot_general x4, matrix products, contract_last(): lax.dot_general(first_op, second_op, (((1,), (1,)), ((), ())), preferred_...  10.5 us
  transfers between devices with their start and end apart: 5, of which 5 were waited for; matrix products, arithmetic and copies ran while one was open for 8% of the time, Pallas kernels for 0%

profile of v1, /device:TPU:0, one launch (start us, length us, event | category | flops | bytes accessed | tf_op | source)
XLA Modules:
  0.0 275.1 jit_solution(2423712639898942933)
XLA Ops:
  13.6 2.0 gather_fusion.2
  15.5 2.0 gather_fusion.1
  17.7 21.7 %all_to_all.15 = bf16[8,64,512]{2,1,0:T(8,128)(2,1)} all-to-all(bf16[8,64,512]{2,1,0:T(8,128)(2,1)S(1)} %bitcast.129), channel_id=1, replica_groups=mesh['sp'=8,'tp'=4] {'sp'}, dimensions={0} | all-to-all | bytes 1048576 | tf_op jit(solution)/shard_map/all_to_all | solution.py:145
  39.5 17.6 %all_to_all.16 = bf16[8,64,512]{2,1,0:T(8,128)(2,1)} all-to-all(bf16[8,64,512]{2,1,0:T(8,128)(2,1)S(1)} %bitcast.128), channel_id=1, replica_groups=mesh['sp'=8,'tp'=4] {'sp'}, dimensions={0} | all-to-all | bytes 1048576 | tf_op jit(solution)/shard_map/all_to_all | solution.py:144
  57.4 3.8 %all-gather.8.cloned.1.call-done = bf16[32,64,512]{2,1,0:T(8,128)(2,1)} async-done(((bf16[8,64,512]{2,1,0:T(8,128)(2,1)}), bf16[32,64,512]{2,1,0:T(8,128)(2,1)}) %all-gather.8.cloned.1.call-update) | async-done | bytes 2097168 | tf_op jit(solution)/shard_map/all_gather | solution.py:153
  61.2 3.2 %copy.92 = bf16[8,64,4,512]{3,2,1,0:T(4,128)(2,1)S(1)} copy(bf16[8,64,4,512]{3,1,0,2:T(8,128)(2,1)} %bitcast.132) | data formatting | bytes 4194304 | tf_op jit(solution)/shard_map/reshape | solution.py:153
  65.0 20.3 %all-gather.6.cloned.1.call-done = bf16[8,64,2048]{2,1,0:T(8,128)(2,1)} async-done(((bf16[8,64,512]{2,1,0:T(8,128)(2,1)}), bf16[8,64,2048]{2,1,0:T(8,128)(2,1)}) %all-gather.6.cloned.1.call-update) | async-done | bytes 2097168 | tf_op jit(solution)/shard_map/all_gather | solution.py:152
  85.3 5.2 %fusion.7 = f32[512,896]{1,0:T(8,128)S(1)} fusion(bf16[512,2048]{1,0:T(8,128)(2,1)} %bitcast.151, bf16[1,896,2048]{2,1,0:T(8,128)(2,1)} %param.26), kind=kOutput, calls=%fused_computation.13 | convolution fusion | flops 1879048192 | bytes 7602176 | tf_op jit(solution)/shard_map/dot_general | solution.py:26
  90.6 2.4 fusion.3
  93.3 2.4 multiply_convert_fusion.2
  95.7 2.3 fusion.1
  98.1 4.1 %add_convert_fusion = bf16[512,2048]{1,0:T(8,128)(2,1)} fusion(f32[512,2048]{1,0:T(8,128)S(1)} %fusion.1, bf16[1,896,2048]{2,1,0:T(8,128)(2,1)S(1)} %copy-done.17, f32[512,896]{1,0:T(8,128)S(1)} %fusion.7, f32[512,896]{1,0:T(8,128)S(1)} %get-tuple-element.220, f32[512,896]{1,0:T(8,128)S(1)} %fusion.3), kind=kOutput, calls=%fused_computation.6 | convolution fusion | flops 1885732864 | bytes 15466496 | tf_op jit(solution)/shard_map/dot_general | solution.py:169
  105.7 21.3 %all-reduce.2 = f32[32]{0:T(128)S(1)} all-reduce(f32[32]{0:T(128)S(1)} %dynamic-update-slice), channel_id=4, replica_groups=mesh['sp'=8,'tp'=4] {'sp'}, use_global_device_ids=true, to_apply=%add.2 | all-reduce | flops 32 | bytes 256
  127.7 5.9 %reduce-scatter.3.cloned.1.call-done = bf16[512,512]{1,0:T(8,128)(2,1)} async-done(((bf16[512,2048]{1,0:T(8,128)(2,1)}), bf16[512,512]{1,0:T(8,128)(2,1)}) %reduce-scatter.3.cloned.1.call-update) | async-done | bytes 524304 | tf_op jit(solution)/shard_map/reduce_scatter | solution.py:172
  133.6 5.5 %all-to-all-start.2 = ((bf16[8,64,512]{2,1,0:T(8,128)(2,1)}), bf16[8,64,512]{2,1,0:T(8,128)(2,1)S(1)}, u32[]{:S(2)}, u32[]{:S(2)}) async-start(bf16[8,64,512]{2,1,0:T(8,128)(2,1)} %bitcast.143), calls=%async_computation.3 | async-start | bytes 1048576 | tf_op jit(solution)/shard_map/all_to_all | solution.py:175
  139.2 6.0 %convert_bitcast_fusion.1 = bf16[1,896,2048]{2,1,0:T(8,128)(2,1)} fusion(bf16[512,896]{1,0:T(8,128)(2,1)} %copy-done.24, bf16[512,2048]{1,0:T(8,128)(2,1)} %bitcast.152), kind=kOutput, calls=%fused_computation.18 | convolution fusion | flops 1880883200 | bytes 6684672 | tf_op jit(solution)/shard_map/dot_general | solution.py:32
  145.2 4.0 %convert_bitcast_fusion = bf16[1,896,2048]{2,1,0:T(8,128)(2,1)} fusion(bf16[512,2048]{1,0:T(8,128)(2,1)S(1)} %bitcast.131, f32[512,896]{1,0:T(8,128)S(1)} %copy-done.23, f32[512,896]{1,0:T(8,128)S(1)} %copy-done.21), kind=kOutput, calls=%fused_computation.17 | convolution fusion | flops 1883635712 | bytes 9437184 | tf_op jit(solution)/shard_map/dot_general | solution.py:32
  149.2 4.3 %all-to-all-done.2 = bf16[8,64,512]{2,1,0:T(8,128)(2,1)S(1)} async-done(((bf16[8,64,512]{2,1,0:T(8,128)(2,1)}), bf16[8,64,512]{2,1,0:T(8,128)(2,1)S(1)}, u32[]{:S(2)}, u32[]{:S(2)}) %all-to-all-start.2) | async-done | bytes 524320 | tf_op jit(solution)/shard_map/all_to_all | solution.py:175
  155.5 5.9 %psum.7 = f32[128]{0:T(128)S(1)} all-reduce(f32[128]{0:T(128)S(1)} %multiply_reduce_fusion), channel_id=1, replica_groups=mesh['sp'=8,'tp'=4] {'tp'}, use_global_device_ids=true, to_apply=%region_8.10 | all-reduce | flops 128 | bytes 1024 | tf_op jit(solution)/shard_map/psum | solution.py:183
  161.6 6.6 %all_gather.25 = bf16[128,2048]{1,0:T(8,128)(2,1)S(1)} all-gather(bf16[128,512]{1,0:T(8,128)(2,1)S(1)} %add_convert_fusion.1), channel_id=1, replica_groups=mesh['sp'=8,'tp'=4] {'tp'}, dimensions={1}, use_global_device_ids=true | all-gather | bytes 655360 | tf_op jit(solution)/shard_map/all_gather | solution.py:188
  169.1 32.9 %all-gather.1 = f32[32,64,64]{2,1,0:T(8,128)S(1)} all-gather(f32[4,64,64]{2,1,0:T(8,128)S(1)} %fusion.30), channel_id=3, replica_groups=mesh['sp'=8,'tp'=4] {'sp'}, dimensions={0}, use_global_device_ids=true | all-gather | bytes 589824 | tf_op jit(solution)/shard_map/all_gather | solution.py:9
  201.9 1.4 convolution_convert_fusion
  208.6 58.3 %reduce-scatter.5.cloned.1.call-done = bf16[256,256]{1,0:T(8,128)(2,1)} async-done(((bf16[2048,256]{1,0:T(8,128)(2,1)}), bf16[256,256]{1,0:T(8,128)(2,1)}) %reduce-scatter.5.cloned.1.call-update) | async-done | bytes 131088 | tf_op jit(solution)/shard_map/reduce_scatter | solution.py:215
  266.9 1.6 convert_element_type.93
  (144 shorter events, 20.0 us)
Async XLA Ops:
  7.2 161.0 %copy-start = (bf16[256,2048]{1,0:T(8,128)(2,1)S(1)}, bf16[256,2048]{1,0:T(8,128)(2,1)}, u32[]{:S(2)}) copy-start(bf16[256,2048]{1,0:T(8,128)(2,1)} %param.35) | copy-start | bytes 3145732
  7.2 6.0 %copy-start.14 = (f32[128,2]{0,1:T(2,128)S(1)}, f32[128,2]{0,1:T(2,128)}, u32[]{:S(2)}) copy-start(f32[128,2]{0,1:T(2,128)} %param.25) | copy-start | bytes 3076
  7.2 54.0 %all-gather.8.cloned.1.call-start = ((), (), s32[]{:S(2)}) async-start(), calls=%async_computation.8 | async-start | bytes 2621440 | tf_op jit(solution)/shard_map/all_gather | solution.py:153
  39.4 45.9 %all-gather.6.cloned.1.call-start = ((), (), s32[]{:S(2)}) async-start(), calls=%async_computation.5 | async-start | bytes 2621440 | tf_op jit(solution)/shard_map/all_gather | solution.py:152
  57.1 76.5 %reduce-scatter.3.cloned.1.call-start = ((), (), s32[]{:S(2)}) async-start(), calls=%async_computation.6 | async-start | bytes 2621440 | tf_op jit(solution)/shard_map/reduce_scatter | solution.py:172
  65.0 28.0 %copy-start.1 = (bf16[64,8,4,512]{3,1,2,0:T(8,128)(2,1)}, bf16[64,8,4,512]{3,1,2,0:T(8,128)(2,1)S(1)}, u32[]{:S(2)}) copy-start(bf16[64,8,4,512]{3,1,2,0:T(8,128)(2,1)S(1)} %copy.105) | copy-start | bytes 6291460
  85.3 5.2 %copy-start.16 = (bf16[1,896,2048]{2,1,0:T(8,128)(2,1)S(1)}, bf16[1,896,2048]{2,1,0:T(8,128)(2,1)}, u32[]{:S(2)}) copy-start(bf16[1,896,2048]{2,1,0:T(8,128)(2,1)} %param.27) | copy-start | bytes 11010052
  85.3 5.2 %copy-start.18 = (bf16[8,64,2048]{2,1,0:T(8,128)(2,1)S(1)}, bf16[8,64,2048]{2,1,0:T(8,128)(2,1)}, u32[]{:S(2)}) copy-start(bf16[8,64,2048]{2,1,0:T(8,128)(2,1)} %all-gather.6.cloned.1.call-done) | copy-start | bytes 6291460
  90.6 7.5 %copy-start.20 = (f32[512,896]{1,0:T(8,128)}, f32[512,896]{1,0:T(8,128)S(1)}, u32[]{:S(2)}) copy-start(f32[512,896]{1,0:T(8,128)S(1)} %fusion.7) | copy-start | bytes 5505028
  90.6 2.7 copy-start.15
  93.0 5.1 %copy-start.22 = (f32[512,896]{1,0:T(8,128)}, f32[512,896]{1,0:T(8,128)S(1)}, u32[]{:S(2)}) copy-start(f32[512,896]{1,0:T(8,128)S(1)} %fusion.3) | copy-start | bytes 5505028
  102.2 24.8 %copy-start.9 = (bf16[128,256]{1,0:T(8,128)(2,1)S(1)}, bf16[128,256]{1,0:T(8,128)(2,1)}, u32[]{:S(2)}) copy-start(bf16[128,256]{1,0:T(8,128)(2,1)} %param.30) | copy-start | bytes 196612
  102.3 24.9 %copy-start.10 = (bf16[128,256]{1,0:T(8,128)(2,1)S(1)}, bf16[128,256]{1,0:T(8,128)(2,1)}, u32[]{:S(2)}) copy-start(bf16[128,256]{1,0:T(8,128)(2,1)} %param.31) | copy-start | bytes 196612
  133.6 19.9 %all-to-all-start.2 = ((bf16[8,64,512]{2,1,0:T(8,128)(2,1)}), bf16[8,64,512]{2,1,0:T(8,128)(2,1)S(1)}, u32[]{:S(2)}, u32[]{:S(2)}) async-start(bf16[8,64,512]{2,1,0:T(8,128)(2,1)} %bitcast.143), calls=%async_computation.3 | async-start | bytes 1048576 | tf_op jit(solution)/shard_map/all_to_all | solution.py:175
  139.1 127.8 %reduce-scatter.5.cloned.1.call-start = ((), (), s32[]{:S(2)}) async-start(), calls=%async_computation.7 | async-start | bytes 1179648 | tf_op jit(solution)/shard_map/reduce_scatter | solution.py:215
  139.1 6.0 %copy-start.2 = (bf16[64,8,4,512]{3,1,2,0:T(8,128)(2,1)S(1)}, bf16[64,8,4,512]{3,1,2,0:T(8,128)(2,1)}, u32[]{:S(2)}) copy-start(bf16[64,8,4,512]{3,1,2,0:T(8,128)(2,1)} %copy-done.1) | copy-start | bytes 6291460
  139.2 6.0 %copy-start.21 = (f32[512,896]{1,0:T(8,128)S(1)}, f32[512,896]{1,0:T(8,128)}, u32[]{:S(2)}) copy-start(f32[512,896]{1,0:T(8,128)} %copy-done.20) | copy-start | bytes 5505028
  139.2 6.0 %copy-start.23 = (f32[512,896]{1,0:T(8,128)S(1)}, f32[512,896]{1,0:T(8,128)}, u32[]{:S(2)}) copy-start(f32[512,896]{1,0:T(8,128)} %copy-done.22) | copy-start | bytes 5505028
  149.2 6.2 %copy-start.3 = (bf16[128,512]{1,0:T(8,128)(2,1)S(1)}, bf16[128,512]{1,0:T(8,128)(2,1)}, u32[]{:S(2)}) copy-start(bf16[128,512]{1,0:T(8,128)(2,1)} %param.20) | copy-start | bytes 393220
  149.2 6.2 %copy-start.12 = (f32[128]{0:T(128)S(1)}, f32[128]{0:T(128)}, u32[]{:S(2)}) copy-start(f32[128]{0:T(128)} %param.22) | copy-start | bytes 1540
  149.2 12.3 %copy-start.4 = (bf16[128,512]{1,0:T(8,128)(2,1)S(1)}, bf16[128,512]{1,0:T(8,128)(2,1)}, u32[]{:S(2)}) copy-start(bf16[128,512]{1,0:T(8,128)(2,1)} %param.21) | copy-start | bytes 393220
  161.5 40.5 %copy-start.7 = (bf16[128,256]{1,0:T(8,128)(2,1)S(1)}, bf16[128,256]{1,0:T(8,128)(2,1)}, u32[]{:S(2)}) copy-start(bf16[128,256]{1,0:T(8,128)(2,1)} %param.32) | copy-start | bytes 196612
  161.6 41.7 %copy-start.5 = (bf16[128,512]{1,0:T(8,128)(2,1)}, bf16[128,512]{1,0:T(8,128)(2,1)S(1)}, u32[]{:S(2)}) copy-start(bf16[128,512]{1,0:T(8,128)(2,1)S(1)} %add_convert_fusion.1) | copy-start | bytes 393220
  203.4 3.9 %copy-start.6 = (f32[1,4,64,64]{3,2,1,0:T(8,128)S(1)}, f32[1,4,64,64]{3,2,1,0:T(8,128)}, u32[]{:S(2)}) copy-start(f32[1,4,64,64]{3,2,1,0:T(8,128)} %param.34) | copy-start | bytes 196612
  (6 other events, 9.9 us)
Sparse Core Ops, SparseCore 0:
  39.6 21.5 all-gather.7
  62.7 22.5 all-gather.5
  102.4 31.1 reduce-scatter.2
  203.5 63.3 reduce-scatter.4
